TPU v7x, 32 devices: a whole 2x2x4 slice. The times are simulated.
32 devices in a mesh: sp: 8 (over z, y), tp: 4 (over x, core).
Axes of the slice: x: 2, y: 2, z: 4, core: 2. Of those that a mesh axis runs over, the one named last changes fastest.
Arguments:
- resid: bfloat16 [2048, 2048], P(('sp', 'tp')), may hold values from -0.21875 to 0.21875
- query_a: bfloat16 [2048, 1024], P('sp', 'tp'), may hold values from -6 to 6
- key_a: bfloat16 [2048, 256], P('sp', 'tp'), may hold values from -6 to 6
- value_a: bfloat16 [2048, 256], P('sp', 'tp'), may hold values from -6 to 6
- query_b: bfloat16 [2048, 1024], P('sp', 'tp'), may hold values from -6 to 6
- key_b: bfloat16 [2048, 512], P('sp', 'tp'), may hold values from -6 to 6
- value_b: bfloat16 [2048, 512], P('sp', 'tp'), may hold values from -6 to 6
- gain_qa: float32 [64], replicated, may hold values from 0.1 to 8
- gain_ka: float32 [64], replicated, may hold values from 0.1 to 8
- gain_qb: float32 [128], replicated, may hold values from 0.1 to 8
- gain_kb: float32 [128], replicated, may hold values from 0.1 to 8
- w_out_a: bfloat16 [1024, 2048], P('tp'), may hold values from -0.125 to 0.125
- w_out_b: bfloat16 [1024, 2048], P('tp'), may hold values from -0.125 to 0.125
- norm_gain: float32 [2048], replicated, may hold values from 0.1 to 1.9
- w_up: bfloat16 [2048, 8192], P('sp', 'tp'), may hold values from -0.125 to 0.125
- w_down: bfloat16 [8192, 2048], P('tp', 'sp'), may hold values from -0.0625 to 0.0625
Outputs:
- result: bfloat16 [2048, 2048], P(('sp', 'tp'))
All inputs are finite; a program needn't handle non-finite values.
Results may differ from a plain program's by a relative error of at most 0.02.
The roundings to bfloat16 on the way count: a program that leaves them out, or rounds other values in their place, can miss the bound.
Values may be sent and summed in bfloat16 or wider, within the bound.
A program may use at most 128 MiB of HBM per device.

v0:
```python
import math

import jax
import jax.numpy as jnp
from jax import lax
from jax.experimental import pallas as pl
from jax.experimental.pallas import tpu as pltpu
from jax.sharding import PartitionSpec as P

GRID_W = 64


EPS = 1e-06


def norm_rope(values, gain, places):
    width = gain.shape[0]
    count = values.shape[0]
    flat = values.astype(jnp.float32).reshape(count, -1, width)
    flat = flat * lax.rsqrt(jnp.mean(flat * flat, axis=-1, keepdims=True) + EPS) * gain
    grid_rows = (places // GRID_W).astype(jnp.float32)
    grid_cols = (places % GRID_W).astype(jnp.float32)
    quarter = width // 4
    freqs = 10000.0 ** (-(2.0 * jnp.arange(quarter, dtype=jnp.float32)) / (width // 2))
    ang_r = grid_rows[:, None] * freqs
    ang_c = grid_cols[:, None] * freqs
    angles = jnp.concatenate([ang_r, ang_r, ang_c, ang_c], axis=-1)
    one, two, three, four = jnp.split(flat, 4, axis=-1)
    turned = jnp.concatenate([-two, one, -four, three], axis=-1)
    return (flat * jnp.cos(angles)[:, None, :] + turned * jnp.sin(angles)[:, None, :]).astype(
        jnp.bfloat16
    )


def fold_block(state, queries, key_block, value_block, scale):
    running, total, accum = state
    scores = (
        jnp.einsum("rkgd,pkd->kgrp", queries, key_block, preferred_element_type=jnp.float32) * scale
    )
    newest = jnp.maximum(running, jnp.max(scores, axis=-1))
    factor = jnp.exp(running - newest)
    expo = jnp.exp(scores - newest[..., None])
    total = total * factor + jnp.sum(expo, axis=-1)
    accum = accum * factor[..., None] + jnp.einsum(
        "kgrp,pkd->kgrd", expo.astype(jnp.bfloat16), value_block, preferred_element_type=jnp.float32
    )
    return (newest, total, accum)


def sweep_keys(state, queries, key_piece, value_piece, scale):
    length = key_piece.shape[0]
    block = math.gcd(length, 2048)
    blocks = length // block
    if blocks == 1:
        return fold_block(state, queries, key_piece, value_piece, scale)
    key_blocks = key_piece.reshape((blocks, block) + key_piece.shape[1:])
    value_blocks = value_piece.reshape((blocks, block) + value_piece.shape[1:])

    def advance(carry, pair):
        return (fold_block(carry, queries, pair[0], pair[1], scale), None)

    state, unused = lax.scan(advance, state, (key_blocks, value_blocks))
    return state


def start_state(queries):
    shape = (queries.shape[1], queries.shape[2], queries.shape[0])
    return (
        jnp.full(shape, -1e30, jnp.float32),
        jnp.zeros(shape, jnp.float32),
        jnp.zeros(shape + (queries.shape[3],), jnp.float32),
    )


def finish(state):
    running, total, accum = state
    outputs = accum / total[..., None]
    count = outputs.shape[2]
    return jnp.transpose(outputs, (2, 0, 1, 3)).reshape(count, -1).astype(jnp.bfloat16)


def local(
    resid,
    query_a,
    key_a,
    value_a,
    query_b,
    key_b,
    value_b,
    gain_qa,
    gain_ka,
    gain_qb,
    gain_kb,
    w_out_a,
    w_out_b,
    norm_gain,
    w_up,
    w_down,
):
    count = query_a.shape[0]
    width_a = gain_qa.shape[0]
    width_b = gain_qb.shape[0]
    places = lax.axis_index("sp") * count + jnp.arange(count, dtype=jnp.int32)
    keys_a = norm_rope(key_a, gain_ka, places)
    keys_b = norm_rope(key_b, gain_kb, places)
    heads_kv_a = keys_a.shape[1]
    heads_kv_b = keys_b.shape[1]
    queries_a = norm_rope(query_a, gain_qa, places)
    queries_b = norm_rope(query_b, gain_qb, places)
    queries_a = queries_a.reshape(count, heads_kv_a, queries_a.shape[1] // heads_kv_a, width_a)
    queries_b = queries_b.reshape(count, heads_kv_b, queries_b.shape[1] // heads_kv_b, width_b)
    values_a = value_a.reshape(count, heads_kv_a, width_a)
    values_b = value_b.reshape(count, heads_kv_b, width_b)
    state_a = sweep_keys(
        start_state(queries_a),
        queries_a,
        lax.all_gather(keys_a, "sp", axis=0, tiled=True),
        lax.all_gather(values_a, "sp", axis=0, tiled=True),
        width_a ** (-0.5),
    )
    state_b = sweep_keys(
        start_state(queries_b),
        queries_b,
        lax.all_gather(keys_b, "sp", axis=0, tiled=True),
        lax.all_gather(values_b, "sp", axis=0, tiled=True),
        width_b ** (-0.5),
    )
    attn_a = finish(state_a)
    attn_b = finish(state_b)
    rows_a, rows_b = (
        lax.all_to_all(attn_a, "tp", split_axis=0, concat_axis=1, tiled=True),
        lax.all_to_all(attn_b, "tp", split_axis=0, concat_axis=1, tiled=True),
    )
    whole_a, whole_b = (
        lax.all_gather(w_out_a, "tp", axis=0, tiled=True),
        lax.all_gather(w_out_b, "tp", axis=0, tiled=True),
    )
    proj = jnp.dot(rows_a, whole_a, preferred_element_type=jnp.float32) + jnp.dot(
        rows_b, whole_b, preferred_element_type=jnp.float32
    )
    mid = (resid.astype(jnp.float32) + proj).astype(jnp.bfloat16)
    midf = mid.astype(jnp.float32)
    normed = (
        midf * lax.rsqrt(jnp.mean(midf * midf, axis=-1, keepdims=True) + EPS) * norm_gain
    ).astype(jnp.bfloat16)
    up_whole, down_whole = (
        lax.all_gather(w_up, "sp", axis=0, tiled=True),
        lax.all_gather(w_down, "sp", axis=1, tiled=True),
    )
    hidden = jnp.square(
        jax.nn.relu(
            jnp.dot(
                lax.all_gather(normed, "tp", axis=0, tiled=True),
                up_whole,
                preferred_element_type=jnp.float32,
            )
        )
    ).astype(jnp.bfloat16)
    mixed = lax.psum_scatter(
        jnp.dot(hidden, down_whole, preferred_element_type=jnp.float32).astype(jnp.bfloat16),
        "tp",
        scatter_dimension=0,
        tiled=True,
    ).astype(jnp.float32)
    return (midf + mixed).astype(jnp.bfloat16)


MESH = pl.DeviceIdType.MESH
INNER = 2
LANES = 128


def remote(src, dst, send, recv, target):
    return pltpu.make_async_remote_copy(
        src_ref=src,
        dst_ref=dst,
        send_sem=send,
        recv_sem=recv,
        device_id=target,
        device_id_type=MESH,
    )


def greet(targets):
    barrier = pltpu.get_barrier_semaphore()
    for target in targets:
        pl.semaphore_signal(barrier, inc=1, device_id=target, device_id_type=MESH)
    pl.semaphore_wait(barrier, len(targets))


def flip(place, k):
    bit = 1
    while bit <= k:
        if k & bit:
            place = place + bit - 2 * bit * lax.rem(place // bit, 2)
        bit *= 2
    return place


def peers_of(place, count):
    return [flip(place, k) for k in range(count - 1, 0, -1)]


def arrive(dst, sem):
    pltpu.make_async_copy(dst, dst, sem).wait()


def front_kernel(
    outer,
    lanes,
    scales,
    k_a,
    v_a,
    k_b,
    v_b,
    q_a,
    q_b,
    cos_a,
    sin_a,
    cos_b,
    sin_b,
    gain_qa,
    gain_ka,
    gain_qb,
    gain_kb,
    resid,
    norm_gain,
    out_a,
    out_b,
    up,
    down,
    up_all,
    down_all,
    mid,
    normed,
    kv,
    kv_all,
    attn,
    part,
    part_in,
    send,
    recv,
    here,
    s_part,
    r_part,
):
    f32 = jnp.float32
    sp = lax.axis_index("sp")
    tp = lax.axis_index("tp")
    z = sp // INNER
    y = sp % INNER
    rows = up.shape[0]
    cols = down.shape[1]
    units = up_all.shape[1]
    count = q_a.shape[0]
    total = outer * INNER
    z_peers = peers_of(z, outer)
    y_peers = peers_of(y, INNER)
    tp_peers = peers_of(tp, lanes)
    greet(
        [{"sp": p * INNER + y} for p in z_peers]
        + [{"sp": z * INNER + p} for p in y_peers]
        + [{"tp": p} for p in tp_peers]
    )
    lane = lax.broadcasted_iota(jnp.int32, (count, LANES), 1)
    low = lane < LANES // 2

    def spin(value, quarter):
        even = lax.rem(lane // quarter, 2) == 0
        ahead = pltpu.roll(value, LANES - quarter, 1)
        behind = pltpu.roll(value, quarter, 1)
        return jnp.where(even, -ahead, behind)

    def turn_b(raw, gain):
        value = raw.astype(f32)
        value = value * lax.rsqrt(jnp.mean(value * value, axis=-1, keepdims=True) + EPS) * gain
        return value * cos_b[...] + spin(value, LANES // 4) * sin_b[...]

    def turn_a(raw, gain):
        value = raw.astype(f32)
        square = value * value
        first = jnp.sum(jnp.where(low, square, 0.0), axis=-1, keepdims=True)
        second = jnp.sum(jnp.where(low, 0.0, square), axis=-1, keepdims=True)
        mean = jnp.where(low, first, second) * (2.0 / LANES)
        value = value * lax.rsqrt(mean + EPS) * gain
        return value * cos_a[...] + spin(value, LANES // 8) * sin_a[...]

    def twice(ref):
        return jnp.concatenate([ref[...], ref[...]], axis=1)

    raw = jnp.concatenate([k_a[...].astype(f32), v_a[...].astype(f32)], axis=1)
    keys = turn_a(raw, twice(gain_ka))
    kv[:, 2 * LANES : 3 * LANES] = jnp.where(low, keys, raw).astype(jnp.bfloat16)
    kv[:, 0:LANES] = turn_b(k_b[...], gain_kb[...]).astype(jnp.bfloat16)
    kv[:, LANES : 2 * LANES] = v_b[...]

    def piece(m, target):
        at = pl.ds(pl.multiple_of(target * units, units), units)
        if m == 0:
            return kv
        return up.at[:, at] if m == 1 else down.at[at, :]

    def place(m, source):
        if m == 0:
            return kv_all.at[source]
        if m == 1:
            return up_all.at[pl.ds(pl.multiple_of(source * rows, rows), rows), :]
        return down_all.at[:, pl.ds(pl.multiple_of(source * cols, cols), cols)]

    started = []

    def ship(m, slot, src, source, target):
        copy = remote(src, place(m, source), send.at[m, slot], recv.at[m, source], target)
        copy.start()
        started.append(copy)

    def open_z(m):
        for i, p in enumerate(z_peers):
            ship(m, i, piece(m, p), sp, {"sp": p * INNER + y})

    def open_y(m):
        for i, p in enumerate(y_peers):
            ship(m, outer - 1 + i, piece(m, z), sp, {"sp": z * INNER + p})

    def forward(m, i):
        source = z_peers[i] * INNER + y
        arrive(place(m, source), recv.at[m, source])
        for n, p in enumerate(y_peers):
            slot = outer - 1 + (i + 1) * (INNER - 1) + n
            ship(m, slot, place(m, source), source, {"sp": z * INNER + p})

    def settle(m):
        for p in y_peers:
            for zs in range(outer):
                source = zs * INNER + p
                arrive(place(m, source), recv.at[m, source])

    own = []
    open_z(0)
    open_y(0)
    for m in (1, 2):
        open_z(m)
    open_y(1)
    for m in range(3):
        copy = pltpu.make_async_copy(piece(m, z), place(m, sp), here.at[m])
        copy.start()
        own.append(copy)
    wide = q_a.shape[1] // LANES
    tall = q_b.shape[1] // LANES
    turned_a = []
    turned_b = []
    for n in range(wide):
        value = turn_a(q_a[:, n * LANES : (n + 1) * LANES], twice(gain_qa))
        other = pltpu.roll(value, LANES // 2, 1)
        for v in (value, other):
            turned_a.append(jnp.where(low, v, 0.0).astype(jnp.bfloat16))
    for n in range(tall):
        value = turn_b(q_b[:, n * LANES : (n + 1) * LANES], gain_qb[...])
        turned_b.append(value.astype(jnp.bfloat16))
    for i in range(outer - 1):
        forward(0, i)
    open_y(2)
    own[0].wait()
    settle(0)

    def attend(query, keys, values, scale):
        scores = lax.dot_general(
            query, keys, (((1,), (1,)), ((), ())), preferred_element_type=f32
        )
        scores = scores * scale
        expo = jnp.exp(scores - jnp.max(scores, axis=-1, keepdims=True))
        summed = jnp.dot(expo.astype(jnp.bfloat16), values, preferred_element_type=f32)
        return summed / jnp.sum(expo, axis=-1, keepdims=True)

    both = kv_all[:, :, 2 * LANES : 3 * LANES].reshape(total * count, LANES)
    for n in range(wide):
        first = attend(turned_a[2 * n], both, both, scales[0])
        second = attend(turned_a[2 * n + 1], both, both, scales[0])
        pair = jnp.where(low, pltpu.roll(first, LANES // 2, 1), second)
        attn[:, n * LANES : (n + 1) * LANES] = pair.astype(jnp.bfloat16)
    forward(1, 0)
    keys = kv_all[:, :, 0:LANES].reshape(total * count, LANES)
    values = kv_all[:, :, LANES : 2 * LANES].reshape(total * count, LANES)
    for n in range(tall):
        made = attend(turned_b[n], keys, values, scales[1])
        attn[:, (wide + n) * LANES : (wide + n + 1) * LANES] = made.astype(jnp.bfloat16)
    split = wide * LANES
    band = resid.shape[0]
    for p in tp_peers + [tp]:
        at = pl.ds(pl.multiple_of(p * band, band), band)
        part[p] = (
            jnp.dot(attn[at, 0:split], out_a[...], preferred_element_type=f32)
            + jnp.dot(attn[at, split:], out_b[...], preferred_element_type=f32)
        ).astype(jnp.bfloat16)
    for i, p in enumerate(tp_peers):
        copy = remote(part.at[p], part_in.at[tp], s_part.at[i], r_part.at[tp], {"tp": p})
        copy.start()
        started.append(copy)
    for i in range(1, outer - 1):
        forward(1, i)
    sums = resid[...].astype(f32) + part[tp].astype(f32)
    for p in tp_peers:
        arrive(part_in.at[p], r_part.at[p])
        sums = sums + part_in[p].astype(f32)
    mid[...] = sums.astype(jnp.bfloat16)
    midf = mid[...].astype(f32)
    norm = lax.rsqrt(jnp.mean(midf * midf, axis=-1, keepdims=True) + EPS)
    normed[...] = (midf * norm * norm_gain[...]).astype(jnp.bfloat16)
    forward(2, 0)

    def close():
        for i in range(1, outer - 1):
            forward(2, i)
        settle(1)
        settle(2)
        for copy in own[1:]:
            copy.wait()

    return close, started


def tail_kernel(
    outer,
    sides,
    close,
    normed,
    mid,
    up,
    down,
    out,
    tokens,
    core_out,
    core_in,
    side_out,
    side_in,
    keep,
    ring_out,
    ring_in,
    s_tok,
    r_tok,
    s_core,
    r_core,
    s_side,
    r_side,
    s_ring,
    r_ring,
):
    sp = lax.axis_index("sp")
    tp = lax.axis_index("tp")
    z = sp // INNER
    y = sp % INNER
    x = tp // INNER
    c = tp % INNER
    lanes = sides * INNER
    rows, width = mid.shape
    f32 = jnp.float32
    z_peers = peers_of(z, outer)
    x_peers = peers_of(x, sides)
    other = 1 - c
    started = []

    def ship(src, dst, send, recv, target):
        copy = remote(src, dst, send, recv, target)
        copy.start()
        started.append(copy)

    sent = [0]

    def pass_on(src, k, lane, target):
        ship(src, tokens.at[k, lane], s_tok.at[sent[0]], r_tok.at[k, lane], target)
        sent[0] += 1

    for k, p in enumerate(z_peers):
        pass_on(normed, k + 1, tp, {"sp": p * INNER + y})
    for p in x_peers:
        pass_on(normed, 0, tp, {"tp": p * INNER + c})
    pass_on(normed, 0, tp, {"tp": x * INNER + other})
    tokens[0, tp] = normed[...]
    close()

    def spread(k):
        arrive(tokens.at[k, tp], r_tok.at[k, tp])
        for p in x_peers:
            pass_on(tokens.at[k, tp], k, tp, {"tp": p * INNER + c})
        pass_on(tokens.at[k, tp], k, tp, {"tp": x * INNER + other})

    def relay(k):
        for p in x_peers:
            lane = p * INNER + c
            arrive(tokens.at[k, lane], r_tok.at[k, lane])
            pass_on(tokens.at[k, lane], k, lane, {"tp": x * INNER + other})

    def complete(k):
        value = keep[k]
        for d in range(sides - 1):
            arrive(side_in.at[k, d], r_side.at[k, d])
            value = value + side_in[k, d].astype(f32)
        if k == 0:
            keep[0] = value
            return
        ring_out[k - 1] = value.astype(jnp.bfloat16)
        target = {"sp": z_peers[k - 1] * INNER + y}
        ship(ring_out.at[k - 1], ring_in.at[k - 1], s_ring.at[k - 1], r_ring.at[k - 1], target)

    for k in range(outer):
        relay(k)
        if k + 1 < outer:
            spread(k + 1)
        for p in range(sides):
            lane = p * INNER + other
            arrive(tokens.at[k, lane], r_tok.at[k, lane])
        block = tokens[k].reshape(lanes * rows, width)
        made = jnp.maximum(jnp.dot(block, up[...], preferred_element_type=f32), 0.0)
        hidden = (made * made).astype(jnp.bfloat16)
        sums = jnp.dot(hidden, down[...], preferred_element_type=f32)
        sums = sums.reshape(sides, INNER, rows, width)
        mine = jnp.where(c == 0, sums[:, 0], sums[:, 1])
        core_out[k] = jnp.where(c == 0, sums[:, 1], sums[:, 0]).astype(jnp.bfloat16)
        ship(core_out.at[k], core_in.at[k], s_core.at[k], r_core.at[k], {"tp": x * INNER + other})
        if k >= 1:
            complete(k - 1)
        arrive(core_in.at[k], r_core.at[k])
        mine = mine + core_in[k].astype(f32)
        side_out[k] = mine.astype(jnp.bfloat16)
        held = mine[0]
        for n in range(1, sides):
            held = jnp.where(x == n, mine[n], held)
        keep[k] = held
        for d, p in enumerate(x_peers):
            ship(
                side_out.at[k, p],
                side_in.at[k, d],
                s_side.at[k, d],
                r_side.at[k, d],
                {"tp": p * INNER + c},
            )
    complete(outer - 1)
    value = mid[...].astype(f32) + keep[0]
    for k in range(outer - 1):
        arrive(ring_in.at[k], r_ring.at[k])
        value = value + ring_in[k].astype(f32)
    out[...] = value.astype(out.dtype)
    for copy in started:
        copy.wait_send()


def layer_kernel(outer, lanes, scales, *refs):
    operands, out, carried = refs[:20], refs[20], refs[21:25]
    close, started = front_kernel(outer, lanes, scales, *operands, *carried, *refs[25:35])
    up_all, down_all, mid, normed = carried
    sides = lanes // INNER
    tail_kernel(outer, sides, close, normed, mid, up_all, down_all, out, *refs[35:])
    for copy in started:
        copy.wait_send()


def layer(operands, total, lanes):
    count = operands[0].shape[0]
    q_a, q_b, resid = operands[4], operands[5], operands[14]
    up, down = operands[18], operands[19]
    outer = total // INNER
    sides = lanes // INNER
    rows, width = resid.shape
    units = up.shape[1] // outer
    kind = jnp.bfloat16
    scales = ((LANES // 2) ** (-0.5), LANES ** (-0.5))
    features = q_a.shape[1] + q_b.shape[1]
    vmem = pl.BlockSpec(memory_space=pltpu.VMEM)
    sems = pltpu.SemaphoreType.DMA
    moves = outer - 1 + outer * (2 * sides - 1)
    near = sides - 1
    far = outer - 1
    carried = [
        pltpu.VMEM((up.shape[0] * total, units), kind),
        pltpu.VMEM((units, down.shape[1] * total), kind),
        pltpu.VMEM(resid.shape, kind),
        pltpu.VMEM(resid.shape, kind),
    ]
    first = [
        pltpu.VMEM((count, 3 * LANES), kind),
        pltpu.VMEM((total, count, 3 * LANES), kind),
        pltpu.VMEM((count, features), kind),
        pltpu.VMEM((lanes, rows, width), kind),
        pltpu.VMEM((lanes, rows, width), kind),
        sems((3, total)),
        sems((3, total)),
        sems((3,)),
        sems((lanes - 1,)),
        sems((lanes,)),
    ]
    second = [
        pltpu.VMEM((outer, lanes, rows, width), kind),
        pltpu.VMEM((outer, sides, rows, width), kind),
        pltpu.VMEM((outer, sides, rows, width), kind),
        pltpu.VMEM((outer, sides, rows, width), kind),
        pltpu.VMEM((outer, near, rows, width), kind),
        pltpu.VMEM((outer, rows, width), jnp.float32),
        pltpu.VMEM((far, rows, width), kind),
        pltpu.VMEM((far, rows, width), kind),
        sems((moves,)),
        sems((outer, lanes)),
        sems((outer,)),
        sems((outer,)),
        sems((outer, near)),
        sems((outer, near)),
        sems((far,)),
        sems((far,)),
    ]
    return pl.pallas_call(
        lambda *refs: layer_kernel(outer, lanes, scales, *refs),
        out_shape=jax.ShapeDtypeStruct(resid.shape, resid.dtype),
        in_specs=[vmem] * 20,
        out_specs=vmem,
        scratch_shapes=carried + first + second,
        compiler_params=pltpu.CompilerParams(
            collective_id=0, has_side_effects=True, vmem_limit_bytes=60 * 1024 * 1024
        ),
        name="layer",
    )(*operands)


def turning_table(places, width, repeat):
    quarter = width // 4
    index = jnp.arange(width * repeat, dtype=jnp.int32) % width
    freqs = 10000.0 ** (-(2.0 * (index % quarter).astype(jnp.float32)) / (width // 2))
    grid = jnp.where(index < width // 2, places[:, None] // GRID_W, places[:, None] % GRID_W)
    angles = grid.astype(jnp.float32) * freqs
    return [jnp.cos(angles), jnp.sin(angles)]


def kernel_local(
    total,
    lanes,
    resid,
    query_a,
    key_a,
    value_a,
    query_b,
    key_b,
    value_b,
    gain_qa,
    gain_ka,
    gain_qb,
    gain_kb,
    w_out_a,
    w_out_b,
    norm_gain,
    w_up,
    w_down,
):
    count = query_a.shape[0]
    places = lax.axis_index("sp") * count + jnp.arange(count, dtype=jnp.int32)
    cos_a, sin_a = turning_table(places, gain_qa.shape[0], 2)
    cos_b, sin_b = turning_table(places, gain_qb.shape[0], 1)
    gains = [g.reshape(1, -1) for g in (gain_qa, gain_ka, gain_qb, gain_kb)]
    operands = [key_a, value_a, key_b, value_b, query_a, query_b, cos_a, sin_a, cos_b, sin_b]
    operands += gains + [resid, norm_gain.reshape(1, -1), w_out_a, w_out_b, w_up, w_down]
    return layer(operands, total, lanes)


def fits(total, lanes, args):
    outer = total // INNER
    sides = lanes // INNER
    if total % INNER or lanes % INNER or outer < 2 or sides < 2:
        return False
    if outer & (outer - 1) or sides & (sides - 1):
        return False
    key_a, key_b, gain_a, gain_b = args[2], args[5], args[7], args[9]
    if 2 * gain_a.shape[0] != LANES or gain_b.shape[0] != LANES:
        return False
    if key_a.shape[1] != lanes * LANES // 2 or key_b.shape[1] != lanes * LANES:
        return False
    if args[1].shape[1] % (lanes * LANES) or args[4].shape[1] % (lanes * LANES):
        return False
    w_up, w_down = args[-2], args[-1]
    units = w_up.shape[1] // lanes // outer
    rows = w_up.shape[0] // total
    cols = w_down.shape[1] // total
    small = units * w_up.shape[0] <= 2**20 and args[0].shape[0] <= 2**11
    return units % LANES == 0 and rows % 16 == 0 and cols % LANES == 0 and small


def sharded(inside, mesh):
    return jax.shard_map(
        inside,
        mesh=mesh,
        in_specs=(
            P(("sp", "tp"), None),
            P("sp", "tp"),
            P("sp", "tp"),
            P("sp", "tp"),
            P("sp", "tp"),
            P("sp", "tp"),
            P("sp", "tp"),
            P(),
            P(),
            P(),
            P(),
            P("tp", None),
            P("tp", None),
            P(),
            P("sp", "tp"),
            P("tp", "sp"),
        ),
        out_specs=P(("sp", "tp"), None),
        check_vma=False,
    )


def solution(mesh):
    total = mesh.shape["sp"]
    lanes = mesh.shape["tp"]

    def run(*args):
        inside = local
        if fits(total, lanes, args):
            inside = lambda *shards: kernel_local(total, lanes, *shards)
        return sharded(inside, mesh)(*args)

    return run
```

profile of v0, /device:TPU:0, one launch (start us, length us, event | category | flops | bytes accessed | tf_op | source)
XLA Modules:
  0.0 148.1 jit_solution(6850154150248296690)
XLA Ops:
  0.0 0.0 copy-start
  0.0 0.7 copy-done
  0.8 0.0 copy-start.1
  0.8 0.7 copy.17.refs_0_
  1.5 0.0 copy-done.1
  1.5 0.7 copy.18.refs_1_
  2.2 1.8 %fusion = (f32[256,128]{1,0:T(8,128)}, f32[256,128]{1,0:T(8,128)}, f32[256,128]{1,0:T(8,128)}, f32[256,128]{1,0:T(8,128)}) fusion(f32[128]{0:T(128)S(1)} %get-tuple-element.14, s32[256]{0:T(256)S(1)} %get-tuple-element.11, s32[256]{0:T(256)S(1)} %get-tuple-element.12, pred[128]{0:T(512)(128)(4,1)S(1)} %get-tuple-element.16, f32[128]{0:T(128)S(1)} %get-tuple-element.13, ...), kind=kLoop, calls=%fused_computation.1 | loop fusion | flops 196608 | bytes 527616 | tf_op jit(solution)/shard_map/sin | solution.py:628
  4.0 142.3 %layer.1 = bf16[64,2048]{1,0:T(8,128)(2,1)} custom-call(bf16[256,64]{1,0:T(8,128)(2,1)} %copy.17.refs_0_, bf16[256,64]{1,0:T(8,128)(2,1)} %copy.18.refs_1_, bf16[256,128]{1,0:T(8,128)(2,1)} %refs_2_.1, bf16[256,128]{1,0:T(8,128)(2,1)} %refs_3_.1, bf16[256,256]{1,0:T(8,128)(2,1)} %refs_4_.1, bf16[256,256]{1,0:T(8,128)(2,1)} %refs_5_.1, ...), custom_call_target="tpu_custom_call" | custom-call | tf_op jit(solution)/shard_map/layer/pallas_call | solution.py:609
  146.4 1.7 %copy.20 = bf16[64,2048]{1,0:T(8,128)(2,1)} copy(bf16[64,2048]{1,0:T(8,128)(2,1)} %layer.1) | data formatting | bytes 524288
  (3 shorter events, 0.0 us)
Async XLA Ops:
  0.0 0.8 copy-start
  0.8 0.8 copy-start.1
where the time goes:
time: 148 us
  Pallas kernels  142 us (96%)
  local copies, waits for them, and re-layouts  3.87 us (3%)
  other arithmetic  1.84 us (1%)
    pallas_call x1, Pallas kernels, layer(): pl.pallas_call(lambda *refs: layer_kernel(outer, lanes, scales, *refs), o...  142 us
    unnamed x7, local copies, waits for them, and re-layouts  3.87 us

commit v1 on v0

v1 whole, which is shorter than its diff:
```python
import math

import jax
import jax.numpy as jnp
import numpy as np
from jax import lax
from jax.experimental import pallas as pl
from jax.experimental.pallas import tpu as pltpu
from jax.sharding import PartitionSpec as P

GRID_W = 64


EPS = 1e-06


def norm_rope(values, gain, places):
    width = gain.shape[0]
    count = values.shape[0]
    flat = values.astype(jnp.float32).reshape(count, -1, width)
    flat = flat * lax.rsqrt(jnp.mean(flat * flat, axis=-1, keepdims=True) + EPS) * gain
    grid_rows = (places // GRID_W).astype(jnp.float32)
    grid_cols = (places % GRID_W).astype(jnp.float32)
    quarter = width // 4
    freqs = 10000.0 ** (-(2.0 * jnp.arange(quarter, dtype=jnp.float32)) / (width // 2))
    ang_r = grid_rows[:, None] * freqs
    ang_c = grid_cols[:, None] * freqs
    angles = jnp.concatenate([ang_r, ang_r, ang_c, ang_c], axis=-1)
    one, two, three, four = jnp.split(flat, 4, axis=-1)
    turned = jnp.concatenate([-two, one, -four, three], axis=-1)
    return (flat * jnp.cos(angles)[:, None, :] + turned * jnp.sin(angles)[:, None, :]).astype(
        jnp.bfloat16
    )


def fold_block(state, queries, key_block, value_block, scale):
    running, total, accum = state
    scores = (
        jnp.einsum("rkgd,pkd->kgrp", queries, key_block, preferred_element_type=jnp.float32) * scale
    )
    newest = jnp.maximum(running, jnp.max(scores, axis=-1))
    factor = jnp.exp(running - newest)
    expo = jnp.exp(scores - newest[..., None])
    total = total * factor + jnp.sum(expo, axis=-1)
    accum = accum * factor[..., None] + jnp.einsum(
        "kgrp,pkd->kgrd", expo.astype(jnp.bfloat16), value_block, preferred_element_type=jnp.float32
    )
    return (newest, total, accum)


def sweep_keys(state, queries, key_piece, value_piece, scale):
    length = key_piece.shape[0]
    block = math.gcd(length, 2048)
    blocks = length // block
    if blocks == 1:
        return fold_block(state, queries, key_piece, value_piece, scale)
    key_blocks = key_piece.reshape((blocks, block) + key_piece.shape[1:])
    value_blocks = value_piece.reshape((blocks, block) + value_piece.shape[1:])

    def advance(carry, pair):
        return (fold_block(carry, queries, pair[0], pair[1], scale), None)

    state, unused = lax.scan(advance, state, (key_blocks, value_blocks))
    return state


def start_state(queries):
    shape = (queries.shape[1], queries.shape[2], queries.shape[0])
    return (
        jnp.full(shape, -1e30, jnp.float32),
        jnp.zeros(shape, jnp.float32),
        jnp.zeros(shape + (queries.shape[3],), jnp.float32),
    )


def finish(state):
    running, total, accum = state
    outputs = accum / total[..., None]
    count = outputs.shape[2]
    return jnp.transpose(outputs, (2, 0, 1, 3)).reshape(count, -1).astype(jnp.bfloat16)


def local(
    resid,
    query_a,
    key_a,
    value_a,
    query_b,
    key_b,
    value_b,
    gain_qa,
    gain_ka,
    gain_qb,
    gain_kb,
    w_out_a,
    w_out_b,
    norm_gain,
    w_up,
    w_down,
):
    count = query_a.shape[0]
    width_a = gain_qa.shape[0]
    width_b = gain_qb.shape[0]
    places = lax.axis_index("sp") * count + jnp.arange(count, dtype=jnp.int32)
    keys_a = norm_rope(key_a, gain_ka, places)
    keys_b = norm_rope(key_b, gain_kb, places)
    heads_kv_a = keys_a.shape[1]
    heads_kv_b = keys_b.shape[1]
    queries_a = norm_rope(query_a, gain_qa, places)
    queries_b = norm_rope(query_b, gain_qb, places)
    queries_a = queries_a.reshape(count, heads_kv_a, queries_a.shape[1] // heads_kv_a, width_a)
    queries_b = queries_b.reshape(count, heads_kv_b, queries_b.shape[1] // heads_kv_b, width_b)
    values_a = value_a.reshape(count, heads_kv_a, width_a)
    values_b = value_b.reshape(count, heads_kv_b, width_b)
    state_a = sweep_keys(
        start_state(queries_a),
        queries_a,
        lax.all_gather(keys_a, "sp", axis=0, tiled=True),
        lax.all_gather(values_a, "sp", axis=0, tiled=True),
        width_a ** (-0.5),
    )
    state_b = sweep_keys(
        start_state(queries_b),
        queries_b,
        lax.all_gather(keys_b, "sp", axis=0, tiled=True),
        lax.all_gather(values_b, "sp", axis=0, tiled=True),
        width_b ** (-0.5),
    )
    attn_a = finish(state_a)
    attn_b = finish(state_b)
    rows_a, rows_b = (
        lax.all_to_all(attn_a, "tp", split_axis=0, concat_axis=1, tiled=True),
        lax.all_to_all(attn_b, "tp", split_axis=0, concat_axis=1, tiled=True),
    )
    whole_a, whole_b = (
        lax.all_gather(w_out_a, "tp", axis=0, tiled=True),
        lax.all_gather(w_out_b, "tp", axis=0, tiled=True),
    )
    proj = jnp.dot(rows_a, whole_a, preferred_element_type=jnp.float32) + jnp.dot(
        rows_b, whole_b, preferred_element_type=jnp.float32
    )
    mid = (resid.astype(jnp.float32) + proj).astype(jnp.bfloat16)
    midf = mid.astype(jnp.float32)
    normed = (
        midf * lax.rsqrt(jnp.mean(midf * midf, axis=-1, keepdims=True) + EPS) * norm_gain
    ).astype(jnp.bfloat16)
    up_whole, down_whole = (
        lax.all_gather(w_up, "sp", axis=0, tiled=True),
        lax.all_gather(w_down, "sp", axis=1, tiled=True),
    )
    hidden = jnp.square(
        jax.nn.relu(
            jnp.dot(
                lax.all_gather(normed, "tp", axis=0, tiled=True),
                up_whole,
                preferred_element_type=jnp.float32,
            )
        )
    ).astype(jnp.bfloat16)
    mixed = lax.psum_scatter(
        jnp.dot(hidden, down_whole, preferred_element_type=jnp.float32).astype(jnp.bfloat16),
        "tp",
        scatter_dimension=0,
        tiled=True,
    ).astype(jnp.float32)
    return (midf + mixed).astype(jnp.bfloat16)


MESH = pl.DeviceIdType.MESH
INNER = 2
SIDES = 2
LANES = 128
HALVES = 2
FAR = (3, 1, 2)


def remote(src, dst, send, recv, target):
    return pltpu.make_async_remote_copy(
        src_ref=src,
        dst_ref=dst,
        send_sem=send,
        recv_sem=recv,
        device_id=target,
        device_id_type=MESH,
    )


def flip(place, k):
    bit = 1
    while bit <= k:
        if k & bit:
            place = place + bit - 2 * bit * lax.rem(place // bit, 2)
        bit *= 2
    return place


def far_order(outer):
    return FAR if outer == 4 else tuple(range(outer - 1, 0, -1))


def arrive(dst, sem):
    pltpu.make_async_copy(dst, dst, sem).wait()


class Mail:
    def __init__(self, sems):
        self.sems = sems
        self.sent = []

    def ship(self, src, dst, recv, target, when=None):
        send = self.sems.at[len(self.sent)]
        self.sent.append((src, send, when))

        def start():
            remote(src, dst, send, recv, target).start()

        if when is None:
            start()
        else:
            pl.when(when)(start)

    def close(self):
        for src, send, when in self.sent:

            def finish(src=src, send=send):
                arrive(src, send)

            if when is None:
                finish()
            else:
                pl.when(when)(finish)


def layer_kernel(
    outer,
    scales,
    ka_t,
    va_t,
    k_b,
    v_b,
    q_a,
    q_b,
    row_table,
    col_table,
    gain_qa,
    gain_ka,
    gain_qb,
    gain_kb,
    norm_gain,
    resid_hbm,
    out_a_hbm,
    out_b_hbm,
    up,
    down,
    out,
    resid,
    out_a,
    out_b,
    kv_all,
    attn,
    up_all,
    down_all,
    pc_out,
    pc_in,
    px_out,
    px_in,
    mid,
    tokens,
    hidden,
    core_out,
    core_in,
    side_out,
    side_in,
    chain_out,
    chain_in,
    held,
    total_sum,
    s_all,
    s_here,
    r_kv,
    r_up,
    r_down,
    r_pc,
    r_px,
    r_tok,
    r_core,
    r_side,
    r_chain,
):
    f32 = jnp.float32
    bf16 = jnp.bfloat16
    sp = lax.axis_index("sp")
    tp = lax.axis_index("tp")
    z = sp // INNER
    y = sp % INNER
    x = tp // INNER
    c = tp % INNER
    lanes = SIDES * INNER
    rows = up.shape[0]
    units = up_all.shape[1]
    count = q_a.shape[0]
    total = outer * INNER
    band, width = mid.shape
    slab = down_all.shape[2] // total
    mail = Mail(s_all)
    z_far = [flip(z, k) for k in far_order(outer)]
    at_z = [{"sp": p * INNER + y} for p in z_far]
    at_y = {"sp": z * INNER + 1 - y}
    at_x = {"tp": (1 - x) * INNER + c}
    at_c = {"tp": x * INNER + 1 - c}
    x_lane = (1 - x) * INNER + c
    has_above = z < outer - 1
    has_below = z > 0
    above = {"sp": jnp.minimum(z + 1, outer - 1) * INNER + y}
    below = {"sp": jnp.maximum(z - 1, 0) * INNER + y}

    barrier = pltpu.get_barrier_semaphore()
    for target in at_z + [at_y, at_x, at_c]:
        pl.semaphore_signal(barrier, inc=1, device_id=target, device_id_type=MESH)

    here = []

    def fetch(src, dst):
        copy = pltpu.make_async_copy(src, dst, s_here.at[len(here)])
        copy.start()
        here.append(copy)
        return copy

    def up_piece(target):
        return up.at[:, pl.ds(pl.multiple_of(target * units, units), units)]

    def up_place(source):
        return up_all.at[pl.ds(pl.multiple_of(source * rows, rows), rows), :]

    def down_piece(h, target):
        at = pl.ds(pl.multiple_of(target * units, units), units)
        return down.at[at, h * slab : (h + 1) * slab]

    def down_place(h, source):
        return down_all.at[h, :, pl.ds(pl.multiple_of(source * slab, slab), slab)]

    get_out_a = fetch(out_a_hbm, out_a)
    get_out_b = fetch(out_b_hbm, out_b)
    get_resid = fetch(resid_hbm, resid)
    get_up = fetch(up_piece(z), up_place(sp))
    get_down = [fetch(down_piece(h, z), down_place(h, sp)) for h in range(HALVES)]

    lane = lax.broadcasted_iota(jnp.int32, (count, LANES), 1)
    low = lane < LANES // 2
    grid_rows = count // GRID_W
    col_part = col_table[...]
    table = jnp.concatenate(
        [col_part + row_table[pl.ds(sp * grid_rows + r, 1), :] for r in range(grid_rows)], axis=0
    )
    cos_a, sin_a, cos_b, sin_b = [table[:, n * LANES : (n + 1) * LANES] for n in range(4)]

    def spin(value, quarter):
        even = lax.rem(lane // quarter, 2) == 0
        ahead = pltpu.roll(value, LANES - quarter, 1)
        behind = pltpu.roll(value, quarter, 1)
        return jnp.where(even, -ahead, behind)

    def turn_b(raw, gain):
        value = raw.astype(f32)
        value = value * lax.rsqrt(jnp.mean(value * value, axis=-1, keepdims=True) + EPS) * gain
        return value * cos_b + spin(value, LANES // 4) * sin_b

    def turn_a(raw, gain):
        value = raw.astype(f32)
        square = value * value
        first = jnp.sum(jnp.where(low, square, 0.0), axis=-1, keepdims=True)
        second = jnp.sum(jnp.where(low, 0.0, square), axis=-1, keepdims=True)
        mean = jnp.where(low, first, second) * (2.0 / LANES)
        value = value * lax.rsqrt(mean + EPS) * gain
        return value * cos_a + spin(value, LANES // 8) * sin_a

    def twice(ref):
        return jnp.concatenate([ref[...], ref[...]], axis=1)

    raw = jnp.concatenate([ka_t[...].astype(f32), va_t[...].astype(f32)], axis=0).T
    keys = turn_a(raw, twice(gain_ka))
    kv_all[sp, :, 2 * LANES : 3 * LANES] = jnp.where(low, keys, raw).astype(bf16)
    kv_all[sp, :, 0:LANES] = turn_b(k_b[...], gain_kb[...]).astype(bf16)
    kv_all[sp, :, LANES : 2 * LANES] = v_b[...]

    pl.semaphore_wait(barrier, outer + 2)

    def send_kv(source, target, when=None):
        mail.ship(kv_all.at[source], kv_all.at[source], r_kv.at[source], target, when)

    send_kv(sp, above, has_above)
    send_kv(sp, below, has_below)
    send_kv(sp, at_y)

    wide = q_a.shape[1] // LANES
    tall = q_b.shape[1] // LANES
    turned_a = []
    turned_b = []
    for n in range(wide):
        value = turn_a(q_a[:, n * LANES : (n + 1) * LANES], twice(gain_qa))
        other = pltpu.roll(value, LANES // 2, 1)
        for v in (value, other):
            turned_a.append(jnp.where(low, v, 0.0).astype(bf16))
    for n in range(tall):
        value = turn_b(q_b[:, n * LANES : (n + 1) * LANES], gain_qb[...])
        turned_b.append(value.astype(bf16))

    def walk(step, visit):
        for near, far, onward, there in (
            (z >= step, jnp.maximum(z - step, 0), above, has_above),
            (z + step < outer, jnp.minimum(z + step, outer - 1), below, has_below),
        ):
            visit(near, far, onward, jnp.logical_and(near, there))

    def pass_kv(near, far, onward, go):
        source = far * INNER + y

        @pl.when(near)
        def _():
            arrive(kv_all.at[source], r_kv.at[source])

        send_kv(source, onward, go)
        send_kv(source, at_y, near)

    def spread(ends, send):
        for p, target in zip(z_far, at_z):
            edge = jnp.logical_or(p == 0, p == outer - 1)
            send(p, target, edge if ends else jnp.logical_not(edge))

    def send_up(ends):
        def send(p, target, when):
            mail.ship(up_piece(p), up_place(sp), r_up.at[sp], target, when)

        spread(ends, send)

    for step in range(1, outer):
        walk(step, pass_kv)
        if step == max(outer - 2, 1):
            send_up(False)
    mail.ship(up_piece(z), up_place(sp), r_up.at[sp], at_y)

    def forward_up(i):
        source = z_far[i] * INNER + y
        arrive(up_place(source), r_up.at[source])
        mail.ship(up_place(source), up_place(source), r_up.at[source], at_y)

    for k in range(outer):
        source = flip(z, k) * INNER + 1 - y
        arrive(kv_all.at[source], r_kv.at[source])
    send_up(True)
    for h in range(HALVES):
        mail.ship(down_piece(h, z), down_place(h, sp), r_down.at[h, sp], at_y)

    def attend(query, keys, values, scale):
        scores = lax.dot_general(
            query, keys, (((1,), (1,)), ((), ())), preferred_element_type=f32
        )
        scores = scores * scale
        expo = jnp.exp(scores - jnp.max(scores, axis=-1, keepdims=True))
        summed = jnp.dot(expo.astype(bf16), values, preferred_element_type=f32)
        return summed / jnp.sum(expo, axis=-1, keepdims=True)

    both = kv_all[:, :, 2 * LANES : 3 * LANES].reshape(total * count, LANES)
    for n in range(wide):
        first = attend(turned_a[2 * n], both, both, scales[0])
        second = attend(turned_a[2 * n + 1], both, both, scales[0])
        pair = jnp.where(low, pltpu.roll(first, LANES // 2, 1), second)
        attn[:, n * LANES : (n + 1) * LANES] = pair.astype(bf16)
    keys = kv_all[:, :, 0:LANES].reshape(total * count, LANES)
    values = kv_all[:, :, LANES : 2 * LANES].reshape(total * count, LANES)
    for n in range(tall):
        made = attend(turned_b[n], keys, values, scales[1])
        attn[:, (wide + n) * LANES : (wide + n + 1) * LANES] = made.astype(bf16)

    split = wide * LANES
    get_out_a.wait()
    get_out_b.wait()

    def project(p):
        at = pl.ds(pl.multiple_of(p * band, band), band)
        return jnp.dot(attn[at, 0:split], out_a[...], preferred_element_type=f32) + jnp.dot(
            attn[at, split:], out_b[...], preferred_element_type=f32
        )

    for n, side in ((0, 1 - x), (1, x)):
        pc_out[n] = project(side * INNER + 1 - c).astype(bf16)
        mail.ship(pc_out.at[n], pc_in.at[n], r_pc.at[n], at_c)
        if n == 0:
            theirs = project(x_lane)
    arrive(pc_in.at[0], r_pc.at[0])
    px_out[...] = (theirs + pc_in[0].astype(f32)).astype(bf16)
    mail.ship(px_out, px_in, r_px.at[0], at_x)
    get_resid.wait()
    sums = resid[...].astype(f32) + project(tp)
    arrive(pc_in.at[1], r_pc.at[1])
    sums = sums + pc_in[1].astype(f32)
    arrive(px_in, r_px.at[0])
    sums = sums + px_in[...].astype(f32)
    mid[...] = sums.astype(bf16)
    midf = mid[...].astype(f32)
    norm = lax.rsqrt(jnp.mean(midf * midf, axis=-1, keepdims=True) + EPS)
    tokens[z, tp] = (midf * norm * norm_gain[...]).astype(bf16)

    part = band // HALVES

    def some(zz, who, p):
        return tokens.at[zz, who, p * part : (p + 1) * part, :]

    def send_tok(zz, who, p, target, when=None):
        mail.ship(some(zz, who, p), some(zz, who, p), r_tok.at[zz, who, p], target, when)

    for p in range(HALVES):
        send_tok(z, tp, p, above, has_above)
        send_tok(z, tp, p, below, has_below)
        send_tok(z, tp, p, at_x)
    for p in range(HALVES):
        send_tok(z, tp, p, at_c)

    def send_down(ends):
        for h in range(HALVES):

            def send(p, target, when):
                mail.ship(down_piece(h, p), down_place(h, sp), r_down.at[h, sp], target, when)

            spread(ends, send)

    for i in range(outer - 1):
        forward_up(i)

    def relay(near, far, p):
        @pl.when(near)
        def _():
            arrive(some(far, x_lane, p), r_tok.at[far, x_lane, p])

        send_tok(far, x_lane, p, at_c, near)

    always = z >= 0
    for step in range(1, outer):
        for p in range(HALVES):

            def pass_tok(near, far, onward, go):
                @pl.when(near)
                def _():
                    arrive(some(far, tp, p), r_tok.at[far, tp, p])

                send_tok(far, tp, p, onward, go)
                send_tok(far, tp, p, at_x, near)
                send_tok(far, tp, p, at_c, near)

            walk(step, pass_tok)
            if step == 1:
                relay(always, z, p)
            else:
                walk(step - 1, lambda near, far, onward, go: relay(near, far, p))
        if step == 1:
            send_down(False)
        if step == max(outer - 2, 1):
            send_down(True)
    for p in range(HALVES):
        walk(outer - 1, lambda near, far, onward, go: relay(near, far, p))

    def forward_down(h, i):
        source = z_far[i] * INNER + y
        arrive(down_place(h, source), r_down.at[h, source])
        mail.ship(down_place(h, source), down_place(h, source), r_down.at[h, source], at_y)

    get_up.wait()
    for k in range(outer):
        source = flip(z, k) * INNER + 1 - y
        arrive(up_place(source), r_up.at[source])
    for k in range(outer):
        zz = flip(z, k)
        for side in range(SIDES):
            who = side * INNER + 1 - c
            for p in range(HALVES):
                arrive(some(zz, who, p), r_tok.at[zz, who, p])
        block = tokens[zz].reshape(lanes * band, width)
        made = jnp.maximum(jnp.dot(block, up_all[...], preferred_element_type=f32), 0.0)
        hidden[zz] = (made * made).astype(bf16)

    inner = jnp.logical_and(z > 0, z < outer - 1)
    order = list(range(outer - 1, -1, -1))
    mixed = [k for k in order if k not in (outer - 1, 0)] + [outer - 1, 0]
    goals = [jnp.where(inner, flip(z, m), flip(z, k)) for k, m in zip(order, mixed)]

    def compute(h, i):
        n = h * outer + i
        sums = jnp.dot(hidden[goals[i]], down_all[h], preferred_element_type=f32)
        sums = sums.reshape(SIDES, INNER, band, total * slab)
        core_out[n] = jnp.where(c == 0, sums[:, 1], sums[:, 0]).astype(bf16)
        mail.ship(core_out.at[n], core_in.at[n], r_core.at[n], at_c)
        held[i] = jnp.where(c == 0, sums[:, 0], sums[:, 1])

    def exchange(h, i):
        n = h * outer + i
        arrive(core_in.at[n], r_core.at[n])
        mine = held[i] + core_in[n].astype(f32)
        side_out[n] = jnp.where(x == 0, mine[1], mine[0]).astype(bf16)
        mail.ship(side_out.at[n], side_in.at[n], r_side.at[n], at_x)
        total_sum[n] = jnp.where(x == 0, mine[0], mine[1])

    def gather(h, i):
        n = h * outer + i
        arrive(side_in.at[n], r_side.at[n])
        total_sum[n] = total_sum[n] + side_in[n].astype(f32)
        goal = goals[i]
        if i == outer - 1:
            for slot, there in ((z, has_below), (outer, has_above)):

                @pl.when(there)
                def _():
                    arrive(chain_in.at[h, slot], r_chain.at[h, slot])
                    total_sum[n] = total_sum[n] + chain_in[h, slot].astype(f32)

            for j in range(total):
                at = slice((j * HALVES + h) * slab, (j * HALVES + h + 1) * slab)
                value = mid[:, at].astype(f32) + total_sum[n, :, j * slab : (j + 1) * slab]
                out[:, at] = value.astype(out.dtype)
            return
        rising = goal > z
        fed = jnp.where(rising, z > 0, z < outer - 1)

        @pl.when(fed)
        def _():
            arrive(chain_in.at[h, goal], r_chain.at[h, goal])
            total_sum[n] = total_sum[n] + chain_in[h, goal].astype(f32)

        chain_out[n] = total_sum[n].astype(bf16)
        step = jnp.where(rising, z + 1, z - 1)
        slot = jnp.where(jnp.logical_and(step == goal, goal < z), outer, goal)
        target = {"sp": step * INNER + y}
        mail.ship(chain_out.at[n], chain_in.at[h, slot], r_chain.at[h, slot], target)

    def settle(h):
        get_down[h].wait()
        for k in range(outer):
            source = flip(z, k) * INNER + 1 - y
            arrive(down_place(h, source), r_down.at[h, source])

    def start_half(h):
        settle(h)
        for i in range(outer):
            compute(h, i)
        for i in range(outer):
            exchange(h, i)

    for i in range(outer - 1):
        forward_down(0, i)
    start_half(0)
    for i in range(outer - 1):
        forward_down(1, i)
    for i in range(2):
        gather(0, i)
    start_half(1)
    for i in range(2, outer):
        gather(0, i)
    for i in range(outer):
        gather(1, i)
    mail.close()


def layer(operands, total, lanes):
    q_a, q_b, resid = operands[4], operands[5], operands[13]
    up, down = operands[16], operands[17]
    count = q_a.shape[0]
    outer = total // INNER
    band, width = resid.shape
    units = up.shape[1] // outer
    kind = jnp.bfloat16
    scales = ((LANES // 2) ** (-0.5), LANES ** (-0.5))
    features = q_a.shape[1] + q_b.shape[1]
    vmem = pl.BlockSpec(memory_space=pltpu.VMEM)
    hbm = pl.BlockSpec(memory_space=pltpu.HBM)
    sems = pltpu.SemaphoreType.DMA
    slab = down.shape[1] // HALVES
    broad = slab * total
    items = outer * HALVES
    scratch = [
        pltpu.VMEM(resid.shape, kind),
        pltpu.VMEM(operands[14].shape, kind),
        pltpu.VMEM(operands[15].shape, kind),
        pltpu.VMEM((total, count, 3 * LANES), kind),
        pltpu.VMEM((count, features), kind),
        pltpu.VMEM((up.shape[0] * total, units), kind),
        pltpu.VMEM((HALVES, units, broad), kind),
        pltpu.VMEM((2, band, width), kind),
        pltpu.VMEM((2, band, width), kind),
        pltpu.VMEM((band, width), kind),
        pltpu.VMEM((band, width), kind),
        pltpu.VMEM((band, width), kind),
        pltpu.VMEM((outer, lanes, band, width), kind),
        pltpu.VMEM((outer, lanes * band, units), kind),
        pltpu.VMEM((items, SIDES, band, broad), kind),
        pltpu.VMEM((items, SIDES, band, broad), kind),
        pltpu.VMEM((items, band, broad), kind),
        pltpu.VMEM((items, band, broad), kind),
        pltpu.VMEM((items, band, broad), kind),
        pltpu.VMEM((HALVES, outer + 1, band, broad), kind),
        pltpu.VMEM((outer, SIDES, band, broad), jnp.float32),
        pltpu.VMEM((items, band, broad), jnp.float32),
        sems((200,)),
        sems((8,)),
        sems((total,)),
        sems((total,)),
        sems((HALVES, total)),
        sems((2,)),
        sems((1,)),
        sems((outer, lanes, HALVES)),
        sems((items,)),
        sems((items,)),
        sems((HALVES, outer + 1)),
    ]
    return pl.pallas_call(
        lambda *refs: layer_kernel(outer, scales, *refs),
        out_shape=jax.ShapeDtypeStruct(resid.shape, resid.dtype),
        in_specs=[vmem] * 13 + [hbm] * 5,
        out_specs=vmem,
        scratch_shapes=scratch,
        compiler_params=pltpu.CompilerParams(
            collective_id=0, has_side_effects=True, vmem_limit_bytes=60 * 1024 * 1024
        ),
        name="layer",
    )(*operands)


def turning_tables(steps, widths, first):
    spots = np.arange(steps, dtype=np.float32)[:, None]
    pieces = []
    for width in widths:
        index = np.arange(LANES) % width
        freqs = (10000.0 ** (-(2.0 * (index % (width // 4))) / (width // 2))).astype(np.float32)
        angles = (spots * freqs).astype(np.float64)
        mine = (index < width // 2) == first
        pieces += [np.where(mine, np.cos(angles), 0.0), np.where(mine, np.sin(angles), 0.0)]
    return jnp.asarray(np.concatenate(pieces, axis=1), jnp.float32)


def kernel_local(
    total,
    lanes,
    resid,
    query_a,
    key_a,
    value_a,
    query_b,
    key_b,
    value_b,
    gain_qa,
    gain_ka,
    gain_qb,
    gain_kb,
    w_out_a,
    w_out_b,
    norm_gain,
    w_up,
    w_down,
):
    widths = (gain_qa.shape[0], gain_qb.shape[0])
    row_table = turning_tables(query_a.shape[0] * total // GRID_W, widths, True)
    col_table = turning_tables(GRID_W, widths, False)
    gains = [g.reshape(1, -1) for g in (gain_qa, gain_ka, gain_qb, gain_kb, norm_gain)]
    operands = [key_a.T, value_a.T, key_b, value_b, query_a, query_b, row_table, col_table]
    operands += gains + [resid, w_out_a, w_out_b, w_up, w_down]
    return layer(operands, total, lanes)


def fits(total, lanes, args):
    outer = total // INNER
    if total % INNER or lanes != INNER * SIDES or outer < 2 or outer & (outer - 1):
        return False
    key_a, key_b, gain_a, gain_b = args[2], args[5], args[7], args[9]
    if 2 * gain_a.shape[0] != LANES or gain_b.shape[0] != LANES:
        return False
    if key_a.shape[1] != lanes * LANES // 2 or key_b.shape[1] != lanes * LANES:
        return False
    if args[1].shape[1] % (lanes * LANES) or args[4].shape[1] % (lanes * LANES):
        return False
    if args[1].shape[0] % (total * GRID_W) or args[0].shape[0] % (total * lanes * HALVES * 16):
        return False
    w_up, w_down = args[-2], args[-1]
    units = w_up.shape[1] // lanes // outer
    rows = w_up.shape[0] // total
    cols = w_down.shape[1] // total
    small = units * w_up.shape[0] <= 2**20 and args[0].shape[0] <= 2**11
    return units % LANES == 0 and rows % 16 == 0 and cols % (HALVES * LANES) == 0 and small


def sharded(inside, mesh):
    return jax.shard_map(
        inside,
        mesh=mesh,
        in_specs=(
            P(("sp", "tp"), None),
            P("sp", "tp"),
            P("sp", "tp"),
            P("sp", "tp"),
            P("sp", "tp"),
            P("sp", "tp"),
            P("sp", "tp"),
            P(),
            P(),
            P(),
            P(),
            P("tp", None),
            P("tp", None),
            P(),
            P("sp", "tp"),
            P("tp", "sp"),
        ),
        out_specs=P(("sp", "tp"), None),
        check_vma=False,
    )


def solution(mesh):
    total = mesh.shape["sp"]
    lanes = mesh.shape["tp"]

    def run(*args):
        inside = local
        if fits(total, lanes, args):
            inside = lambda *shards: kernel_local(total, lanes, *shards)
        return sharded(inside, mesh)(*args)

    return run
```

time: 148 us -> 120 us (0.81)
  Pallas kernels: 142 us -> 118 us
  local copies, waits for them, and re-layouts: 3.87 us -> 1.67 us
  other arithmetic: 1.84 us -> 0 us
    pallas_call x1, Pallas kernels: 142 us -> 118 us  [layer(): pl.pallas_call(lambda *refs: layer_kernel(outer, scales, *refs), out_shap...]
    unnamed x7 -> x1, local copies, waits for them, and re-layouts: 3.87 us -> 1.67 us
    sin x1 -> x0, other arithmetic: 1.81 us -> none  [turning_table(): return [jnp.cos(angles), jnp.sin(angles)]]
where the time goes in v1:
time: 120 us; the launch traced here: 119 us
  Pallas kernels  118 us (98%)
  local copies, waits for them, and re-layouts  1.67 us (1%)
    pallas_call x1, Pallas kernels, layer(): pl.pallas_call(lambda *refs: layer_kernel(outer, scales, *refs), out_shap...  118 us

profile of v1, /device:TPU:0, one launch (start us, length us, event | category | flops | bytes accessed | tf_op | source)
XLA Modules:
  0.0 119.4 jit_solution(9938931327186767189)
XLA Ops:
  0.0 117.7 %layer.1 = bf16[64,2048]{1,0:T(8,128)(2,1)} custom-call(bf16[64,256]{1,0:T(8,128)(2,1)} %bitcast.7, bf16[64,256]{1,0:T(8,128)(2,1)} %bitcast.8, bf16[256,128]{1,0:T(8,128)(2,1)} %refs_2_.1, bf16[256,128]{1,0:T(8,128)(2,1)} %refs_3_.1, bf16[256,256]{1,0:T(8,128)(2,1)} %refs_4_.1, bf16[256,256]{1,0:T(8,128)(2,1)} %refs_5_.1, f32[32,512]{1,0:T(8,128)} %constant.4.clone.refs_6_, ...), custom_call_target="tpu_custom_call" | custom-call | tf_op jit(solution)/shard_map/layer/pallas_call | solution.py:713
  117.7 1.7 %copy.20 = bf16[64,2048]{1,0:T(8,128)(2,1)} copy(bf16[64,2048]{1,0:T(8,128)(2,1)} %layer.1) | data formatting | bytes 524288
